TPU v7x, 32 devices: a whole 2x2x4 slice. The times are simulated.
32 devices in a mesh: ep: 8 (over z, x), tp: 4 (over y, core).
Axes of the slice: x: 2, y: 2, z: 4, core: 2. Of those that a mesh axis runs over, the one named last changes fastest.
Arguments:
- tokens: bfloat16 [256, 2048], P('ep'), may hold values from -24 to 24
- norm_gain: float32 [2048], replicated, may hold values from 0.1 to 1.9
- post_gain: float32 [2048], replicated, may hold values from 0.1 to 1.9
- w_query: bfloat16 [2048, 2048], P(None, 'tp'), may hold values from -0.125 to 0.125
- w_key: bfloat16 [2048, 512], P(None, 'tp'), may hold values from -0.125 to 0.125
- w_value: bfloat16 [2048, 512], P(None, 'tp'), may hold values from -0.125 to 0.125
- w_forget: bfloat16 [2048, 32], replicated, may hold values from -0.25 to 0.25
- w_output: bfloat16 [2048, 2048], P('tp'), may hold values from -0.125 to 0.125
- key_cache: bfloat16 [256, 8, 64, 1024], P('ep', 'tp'), may hold values from -660 to 660
- value_cache: bfloat16 [256, 8, 64, 1024], P('ep', 'tp'), may hold values from -6 to 6
- gate_cache: float32 [256, 32, 1024], P('ep', 'tp'), may hold values from -176.08 to 0, as said below
- lengths: int32 [256], P('ep'), may hold values from 256 to 1024
- routes: int32 [256, 2], P('ep'), may hold values from 0 to 7, all different within a row; in each aligned block of 32 rows (0 to 31, 32 to 63, ...) at most 16 rows name the same one
- route_logits: float32 [256, 2], P('ep'), may hold values from -6 to 6
- w_gate: bfloat16 [8, 2048, 3584], P('ep', None, 'tp'), may hold values from -0.125 to 0.125
- w_up: bfloat16 [8, 2048, 3584], P('ep', None, 'tp'), may hold values from -0.125 to 0.125
- w_down: bfloat16 [8, 3584, 2048], P('ep', 'tp'), may hold values from -0.09375 to 0.09375
Outputs:
- layer_out: bfloat16 [256, 2048], P('ep', 'tp')
Inputs may be any that keep to these rules, and one draw needn't show every extreme that they name: `routes`: each row names 2 different experts. The rows of one index of ep name any one expert at most 16 times, and in every draw some index of ep names some expert exactly 16 times. `gate_cache`: cumulative sums of negative log forget gates along positions: nonincreasing along the last dimension. `lengths`: the new token follows the valid positions of its sequence.
All inputs are finite; a program needn't handle non-finite values.
Results may differ from a plain program's by a relative error of at most 0.011.
Values may be sent and summed in bfloat16 or wider, within the bound.
No kernel may reach another device: no remote copies, remote signals or barrier semaphores. Data moves between devices by JAX's collectives and lax.ppermute only.
A program may use at most 64 MiB of HBM per device.

v0:
```python
import jax
import jax.numpy as jnp
from jax import lax
from jax.sharding import PartitionSpec as P

epsilon = 1e-06


def body(
    tokens,
    norm_gain,
    post_gain,
    w_query,
    w_key,
    w_value,
    w_forget,
    w_output,
    key_cache,
    value_cache,
    gate_cache,
    lengths,
    routes,
    route_logits,
    w_gate,
    w_up,
    w_down,
):
    ep_count = lax.axis_size("ep")
    tp_count = lax.axis_size("tp")
    tp_index = lax.axis_index("tp")
    seq_count, width = tokens.shape
    kv_local, head_dim, cache_span = (key_cache.shape[1], key_cache.shape[2], key_cache.shape[3])
    heads_local = gate_cache.shape[1]
    group_size = heads_local // kv_local
    own_width = width // tp_count
    column_start = tp_index * own_width
    tokens_wide = tokens.astype(jnp.float32)
    normed = (
        tokens_wide
        * lax.rsqrt(jnp.mean(tokens_wide * tokens_wide, axis=-1, keepdims=True) + epsilon)
        * norm_gain
    ).astype(jnp.bfloat16)
    forget_columns = lax.dynamic_slice_in_dim(w_forget, tp_index * heads_local, heads_local, 1)
    log_forget = jax.nn.log_sigmoid(
        jnp.dot(normed, forget_columns, preferred_element_type=jnp.float32)
    )
    query_vector = jnp.dot(normed, w_query, preferred_element_type=jnp.float32).astype(jnp.bfloat16)
    fresh_key = jnp.dot(normed, w_key, preferred_element_type=jnp.float32).astype(jnp.bfloat16)
    value_new = jnp.dot(normed, w_value, preferred_element_type=jnp.float32).astype(jnp.bfloat16)
    query_vector = query_vector.reshape(seq_count, kv_local, group_size, head_dim)
    fresh_key = fresh_key.reshape(seq_count, kv_local, head_dim)
    value_new = value_new.reshape(seq_count, kv_local, head_dim)
    score_scale = head_dim ** (-0.5)
    past_scores = jnp.einsum(
        "bkgd,bkdl->bkgl", query_vector, key_cache, preferred_element_type=jnp.float32
    ).reshape(seq_count, heads_local, cache_span)
    cache_position = lax.broadcasted_iota(jnp.int32, (1, 1, cache_span), 2)
    last_index = (lengths - 1)[:, None, None]
    latest = jnp.sum(jnp.where(cache_position == last_index, gate_cache, 0.0), axis=-1)
    past_scores = past_scores * score_scale + (latest + log_forget)[:, :, None] - gate_cache
    past_scores = jnp.where(cache_position < lengths[:, None, None], past_scores, -jnp.inf)
    new_score = (
        jnp.einsum(
            "rlse,rle->rls", query_vector, fresh_key, preferred_element_type=jnp.float32
        ).reshape(seq_count, heads_local)
        * score_scale
    )
    peak_score = jnp.maximum(jnp.max(past_scores, axis=-1), new_score)
    past_exp = jnp.exp(past_scores - peak_score[:, :, None])
    new_exp = jnp.exp(new_score - peak_score)
    denominator = jnp.sum(past_exp, axis=-1) + new_exp
    past_prob = (past_exp / denominator[:, :, None]).astype(jnp.bfloat16)
    new_prob = (new_exp / denominator).astype(jnp.bfloat16)
    mixed_heads = jnp.einsum(
        "bkgl,bkdl->bkgd",
        past_prob.reshape(seq_count, kv_local, group_size, cache_span),
        value_cache,
        preferred_element_type=jnp.float32,
    )
    mixed_heads = mixed_heads + new_prob.reshape(seq_count, kv_local, group_size)[
        :, :, :, None
    ].astype(jnp.float32) * value_new[:, :, None, :].astype(jnp.float32)
    attended = mixed_heads.astype(jnp.bfloat16).reshape(seq_count, heads_local * head_dim)
    partial_value = jnp.dot(attended, w_output, preferred_element_type=jnp.float32).astype(
        jnp.bfloat16
    )
    attention = lax.psum_scatter(partial_value, "tp", scatter_dimension=1, tiled=True).astype(
        jnp.float32
    )
    residual = lax.dynamic_slice_in_dim(tokens_wide, column_start, own_width, 1) + attention
    squares = lax.psum(jnp.sum(residual * residual, axis=-1), "tp")
    gain_part = lax.dynamic_slice_in_dim(post_gain, column_start, own_width, 0)
    expert_input = (residual * lax.rsqrt(squares / width + epsilon)[:, None] * gain_part).astype(
        jnp.bfloat16
    )
    route_width = routes.shape[1]
    route_count = seq_count * route_width
    capacity = 2 * seq_count * route_width // ep_count
    slot_count = ep_count * capacity
    flat_routes = routes.reshape(route_count)
    expert_onehot = (
        flat_routes[:, None] == lax.broadcasted_iota(jnp.int32, (1, ep_count), 1)
    ).astype(jnp.int32)
    route_rank = jnp.sum(jnp.cumsum(expert_onehot, axis=0) * expert_onehot, axis=1) - 1
    slot_index = flat_routes * capacity + route_rank
    slot_onehot = (
        slot_index[:, None] == lax.broadcasted_iota(jnp.int32, (1, slot_count), 1)
    ).astype(jnp.float32)
    token_onehot = (
        lax.broadcasted_iota(jnp.int32, (route_count, 1), 0) // route_width
        == lax.broadcasted_iota(jnp.int32, (1, seq_count), 1)
    ).astype(jnp.float32)
    dispatch = jnp.dot(slot_onehot.T, token_onehot).astype(jnp.bfloat16)
    packed = jnp.dot(dispatch, expert_input, preferred_element_type=jnp.float32).astype(
        jnp.bfloat16
    )
    sent_width = packed.shape[1]
    arrived = lax.all_to_all(
        packed.reshape(ep_count, capacity, sent_width),
        "ep",
        split_axis=0,
        concat_axis=0,
        tiled=True,
    )
    expert_rows = arrived.reshape(slot_count, sent_width)
    expert_rows = lax.all_gather(expert_rows, "tp", axis=1, tiled=True)
    gate_act = jnp.dot(expert_rows, w_gate[0], preferred_element_type=jnp.float32)
    upper = jnp.dot(expert_rows, w_up[0], preferred_element_type=jnp.float32)
    hidden_act = (jax.nn.silu(gate_act) * upper).astype(jnp.bfloat16)
    down_part = jnp.dot(hidden_act, w_down[0], preferred_element_type=jnp.float32).astype(
        jnp.bfloat16
    )
    expert_out = (
        lax.psum_scatter(down_part, "tp", scatter_dimension=1, tiled=True)
        .astype(jnp.float32)
        .astype(jnp.bfloat16)
    )
    returned = lax.all_to_all(
        expert_out.reshape(ep_count, capacity, own_width),
        "ep",
        split_axis=0,
        concat_axis=0,
        tiled=True,
    )
    route_weight = jax.nn.softmax(route_logits, axis=-1).reshape(route_count)
    combine = jnp.dot(
        token_onehot.T, slot_onehot * route_weight[:, None], precision=lax.Precision.HIGHEST
    )
    expert_mix = jnp.dot(
        combine,
        returned.reshape(slot_count, own_width).astype(jnp.float32),
        precision=lax.Precision.HIGHEST,
    )
    return (residual + expert_mix).astype(jnp.bfloat16)


def solution(mesh):
    in_specs = (
        P("ep", None),
        P(),
        P(),
        P(None, "tp"),
        P(None, "tp"),
        P(None, "tp"),
        P(),
        P("tp", None),
        P("ep", "tp", None, None),
        P("ep", "tp", None, None),
        P("ep", "tp", None),
        P("ep"),
        P("ep", None),
        P("ep", None),
        P("ep", None, "tp"),
        P("ep", None, "tp"),
        P("ep", "tp", None),
    )
    out_specs = P("ep", "tp")
    return jax.shard_map(body, mesh=mesh, in_specs=in_specs, out_specs=out_specs, check_vma=False)
```

profile of v0, /device:TPU:0, one launch (start us, length us, event | category | flops | bytes accessed | tf_op | source)
XLA Modules:
  0.0 132.9 jit_solution(5360184563448234798)
XLA Ops:
  6.5 0.0 copy-start
  6.5 0.0 reduce-scatter.3.cloned.1.call-start
  6.5 0.8 broadcast_add_fusion
  7.3 0.7 iota_compare_fusion.1
  8.1 1.0 multiply_reduce_fusion
  9.1 0.1 iota_compare_fusion
  9.2 1.5 %select_reduce_fusion = f32[32,8]{1,0:T(8,128)S(1)} fusion(f32[32,8,1024]{2,1,0:T(8,128)} %param.27, pred[32,1024]{1,0:T(8,128)(4,1)S(1)} %iota_compare_fusion), kind=kLoop, calls=%fused_computation.25 | loop fusion | flops 524032 | bytes 1082368 | tf_op jit(solution)/shard_map/reduce_sum | solution.py:59
  10.7 0.1 copy.36
  10.8 1.1 fusion.43
  11.9 0.1 copy.37
  12.0 2.2 %convolution_convert_fusion.2 = bf16[32,512]{1,0:T(8,128)(2,1)S(1)} fusion(bf16[2048,512]{1,0:T(8,128)(2,1)} %param.20, f32[2048]{0:T(1024)} %param.18, f32[32]{0:T(128)S(1)} %add_rsqrt_fusion.1, bf16[32,2048]{1,0:T(8,128)(2,1)} %param.17), kind=kOutput, calls=%fused_computation.16 | convolution fusion | flops 67387392 | bytes 2269312 | tf_op jit(solution)/shard_map/dot_general | solution.py:47
  14.2 0.1 reshape.169
  14.3 4.6 %convolution_multiply_fusion = f32[32,2,4,1024]{3,2,1,0:T(4,128)S(1)} fusion(bf16[32,2,4,64]{3,2,1,0:T(4,128)(2,1)S(1)} %reshape.169, bf16[32,2,64,1024]{3,2,1,0:T(8,128)(2,1)} %param.25), kind=kOutput, calls=%fused_computation.8 | convolution fusion | flops 33816576 | bytes 9469952 | tf_op jit(solution)/shard_map/bkgd,bkdl->bkgl/dot_general | solution.py:54
  18.9 0.0 copy-start.3
  18.9 1.4 %mul.121 = f32[32,8,1024]{2,1,0:T(8,128)} reshape(f32[32,2,4,1024]{3,2,1,0:T(4,128)S(1)} %convolution_multiply_fusion) | data formatting | bytes 2097152 | tf_op jit(solution)/shard_map/mul | solution.py:60
  20.3 1.9 %fusion.54 = (f32[32,8]{1,0:T(8,128)S(1)}, f32[32,8,1024]{2,1,0:T(8,128)S(1)}) fusion(f32[32,8,1024]{2,1,0:T(8,128)} %param.27, f32[32,8,1024]{2,1,0:T(8,128)} %mul.121, f32[32,8]{1,0:T(8,128)S(1)} %copy.37, pred[32,1024]{1,0:T(8,128)(4,1)S(1)} %iota_compare_fusion.1), kind=kLoop, calls=%fused_computation.81 | loop fusion | flops 1048320 | bytes 3180544 | tf_op jit(solution)/shard_map/reduce_max | solution.py:68
  22.2 0.1 copy.38
  22.2 0.0 copy-done.1
  22.2 0.0 copy-done.3
  22.2 1.3 convolution_convert_fusion.5
  23.5 0.1 reshape.182
  23.6 0.2 fusion.55
  23.8 0.1 copy.48
  23.9 0.1 copy.39
  24.0 0.3 fusion.18
  24.3 0.1 copy.40
  24.4 0.1 copy.41
  24.5 1.1 divide_convert_fusion
  25.6 1.2 reshape.171
  26.8 0.1 copy.44
  26.9 1.3 fusion.17
  28.2 0.1 reshape.178
  28.3 0.0 copy-start.5
  28.3 5.7 %fusion.15 = bf16[32,2,4,64]{3,2,1,0:T(4,128)(2,1)S(1)} fusion(bf16[32,2,4,1024]{3,2,1,0:T(4,128)(2,1)S(1)} %reshape.171, bf16[32,2,64,1024]{3,2,1,0:T(8,128)(2,1)} %param.26, f32[32,2,64]{2,1,0:T(2,128)S(1)} %reshape.178, f32[32,2,4]{2,1,0:T(2,128)S(1)} %copy.44), kind=kOutput, calls=%fused_computation.13 | convolution fusion | flops 33603584 | bytes 8963072 | tf_op jit(solution)/shard_map/bkgl,bkdl->bkgd/dot_general | solution.py:74
  34.0 0.1 reshape.172
  34.1 0.0 copy-done
  34.1 1.1 convolution_convert_fusion
  35.2 0.0 reduce-scatter.3.cloned.1.call-update
  35.3 0.0 reduce-scatter.5.cloned.1.call-start
  35.3 0.0 copy-done.5
  35.3 0.1 copy.45
  35.4 0.1 reshape.173
  35.5 0.1 fusion.31
  35.6 0.1 reduce_window_sum.11
  35.7 0.2 select_reduce_fusion.1
  35.9 0.8 dynamic_slice.11
  36.7 21.2 %reduce-scatter.3.cloned.1.call-done = bf16[32,512]{1,0:T(8,128)(2,1)} async-done(((bf16[32,2048]{1,0:T(8,128)(2,1)}), bf16[32,512]{1,0:T(8,128)(2,1)}) %reduce-scatter.3.cloned.1.call-update) | async-done | bytes 32784 | tf_op jit(solution)/shard_map/reduce_scatter | solution.py:87
  57.8 0.9 multiply_reduce_fusion.1
  58.7 5.8 %psum.7 = f32[32]{0:T(128)S(1)} all-reduce(f32[32]{0:T(128)S(1)} %multiply_reduce_fusion.1), channel_id=1, replica_groups=mesh['ep'=8,'tp'=4] {'tp'}, use_global_device_ids=true, to_apply=%region_10.11 | all-reduce | flops 32 | bytes 256 | tf_op jit(solution)/shard_map/psum | solution.py:91
  64.5 1.2 convolution_convert_fusion.1
  65.7 12.8 %all_to_all.10 = bf16[8,16,512]{2,1,0:T(8,128)(2,1)S(1)} all-to-all(bf16[8,16,512]{2,1,0:T(8,128)(2,1)S(1)} %bitcast.46), channel_id=1, replica_groups=mesh['ep'=8,'tp'=4] {'ep'}, dimensions={0} | all-to-all | bytes 262144 | tf_op jit(solution)/shard_map/all_to_all | solution.py:118
  78.5 6.5 %all_gather.3 = bf16[128,2048]{1,0:T(8,128)(2,1)S(1)} all-gather(bf16[128,512]{1,0:T(8,128)(2,1)S(1)} %bitcast.43), channel_id=1, replica_groups=mesh['ep'=8,'tp'=4] {'tp'}, dimensions={1}, use_global_device_ids=true | all-gather | bytes 655360 | tf_op jit(solution)/shard_map/all_gather | solution.py:126
  85.0 2.8 %fusion.4 = f32[128,896]{1,0:T(8,128)S(1)} fusion(bf16[128,2048]{1,0:T(8,128)(2,1)S(1)} %all_gather.3, bf16[1,2048,896]{2,1,0:T(8,128)(2,1)} %param.31), kind=kOutput, calls=%fused_computation.4 | convolution fusion | flops 469762048 | bytes 4653056 | tf_op jit(solution)/shard_map/dot_general | solution.py:127
  87.8 0.0 copy-start.4
  87.8 5.3 %fusion.6 = bf16[128,2048]{1,0:T(8,128)(2,1)} fusion(bf16[1,896,2048]{2,1,0:T(8,128)(2,1)} %param.33, bf16[128,2048]{1,0:T(8,128)(2,1)S(1)} %all_gather.3, bf16[1,2048,896]{2,1,0:T(8,128)(2,1)} %param.32, f32[128,896]{1,0:T(8,128)S(1)} %fusion.4), kind=kOutput, calls=%fused_computation.6 | convolution fusion | flops 940474368 | bytes 8847360 | tf_op jit(solution)/shard_map/dot_general | solution.py:130
  93.1 0.0 reduce-scatter.5.cloned.1.call-update
  93.2 19.3 %reduce-scatter.5.cloned.1.call-done = bf16[128,512]{1,0:T(8,128)(2,1)} async-done(((bf16[128,2048]{1,0:T(8,128)(2,1)}), bf16[128,512]{1,0:T(8,128)(2,1)}) %reduce-scatter.5.cloned.1.call-update) | async-done | bytes 131088 | tf_op jit(solution)/shard_map/reduce_scatter | solution.py:134
  112.4 5.5 %all-to-all-start.1 = ((bf16[8,16,512]{2,1,0:T(8,128)(2,1)}), bf16[8,16,512]{2,1,0:T(8,128)(2,1)S(1)}, u32[]{:S(2)}, u32[]{:S(2)}) async-start(bf16[8,16,512]{2,1,0:T(8,128)(2,1)} %bitcast.45), calls=%async_computation.3 | async-start | bytes 262144 | tf_op jit(solution)/shard_map/all_to_all | solution.py:138
  117.9 0.1 copy.46
  118.0 0.1 mul.132
  118.1 0.3 fusion.29
  118.4 6.9 %all-to-all-done.1 = bf16[8,16,512]{2,1,0:T(8,128)(2,1)S(1)} async-done(((bf16[8,16,512]{2,1,0:T(8,128)(2,1)}), bf16[8,16,512]{2,1,0:T(8,128)(2,1)S(1)}, u32[]{:S(2)}, u32[]{:S(2)}) %all-to-all-start.1) | async-done | bytes 131104 | tf_op jit(solution)/shard_map/all_to_all | solution.py:138
  125.3 0.0 copy-done.2
  125.3 0.8 fusion.16
  (14 shorter events, 0.1 us)
Async XLA Ops:
  6.5 27.6 %copy-start = (bf16[512,2048]{1,0:T(8,128)(2,1)S(1)}, bf16[512,2048]{1,0:T(8,128)(2,1)}, u32[]{:S(2)}) copy-start(bf16[512,2048]{1,0:T(8,128)(2,1)} %param.24) | copy-start | bytes 6291460
  6.5 51.3 %reduce-scatter.3.cloned.1.call-start = ((), (), s32[]{:S(2)}) async-start(), calls=%async_computation.4 | async-start | bytes 163840 | tf_op jit(solution)/shard_map/reduce_scatter | solution.py:87
  18.9 3.3 %copy-start.1 = (bf16[32,2048]{1,0:T(8,128)(2,1)S(1)}, bf16[32,2048]{1,0:T(8,128)(2,1)}, u32[]{:S(2)}) copy-start(bf16[32,2048]{1,0:T(8,128)(2,1)} %param.17) | copy-start | bytes 393220
  18.9 3.3 %copy-start.3 = (f32[2048]{0:T(1024)S(1)}, f32[2048]{0:T(1024)}, u32[]{:S(2)}) copy-start(f32[2048]{0:T(1024)} %param.18) | copy-start | bytes 24580
  28.3 7.0 %copy-start.5 = (s32[32,2]{0,1:T(2,128)S(1)}, s32[32,2]{0,1:T(2,128)}, u32[]{:S(2)}) copy-start(s32[32,2]{0,1:T(2,128)} %param.29) | copy-start | bytes 772
  35.3 77.2 %reduce-scatter.5.cloned.1.call-start = ((), (), s32[]{:S(2)}) async-start(), calls=%async_computation.5 | async-start | bytes 655360 | tf_op jit(solution)/shard_map/reduce_scatter | solution.py:134
  87.8 5.3 %copy-start.4 = (f32[32,2]{0,1:T(2,128)S(1)}, f32[32,2]{0,1:T(2,128)}, u32[]{:S(2)}) copy-start(f32[32,2]{0,1:T(2,128)} %param.30) | copy-start | bytes 772
  87.8 37.5 %copy-start.2 = (bf16[32,512]{1,0:T(8,128)(2,1)S(1)}, bf16[32,512]{1,0:T(8,128)(2,1)}, u32[]{:S(2)}) copy-start(bf16[32,512]{1,0:T(8,128)(2,1)} %reduce-scatter.3.cloned.1.call-done) | copy-start | bytes 98308
  112.4 12.8 %all-to-all-start.1 = ((bf16[8,16,512]{2,1,0:T(8,128)(2,1)}), bf16[8,16,512]{2,1,0:T(8,128)(2,1)S(1)}, u32[]{:S(2)}, u32[]{:S(2)}) async-start(bf16[8,16,512]{2,1,0:T(8,128)(2,1)} %bitcast.45), calls=%async_computation.3 | async-start | bytes 262144 | tf_op jit(solution)/shard_map/all_to_all | solution.py:138
Sparse Core Ops, SparseCore 0:
  35.4 22.4 reduce-scatter.2
  93.2 19.1 reduce-scatter.4
where the time goes:
time: 134 us; the launch traced here: 133 us
  waiting for transfers between devices  47.3 us (35%)
  matrix products  27.8 us (21%)
  blocking collectives  25.1 us (19%)
  between operations  13.6 us (10%)
  other arithmetic  8.77 us (7%)
  starting transfers between devices  5.54 us (4%)
  local copies, waits for them, and re-layouts  4.81 us (4%)
    reduce_scatter x1, waiting for transfers between devices, body(): lax.psum_scatter(partial_value, 'tp', scatter_dimension=1, tiled=True)  21.2 us
    reduce_scatter x1, waiting for transfers between devices, body(): lax.psum_scatter(down_part, 'tp', scatter_dimension=1, tiled=True)  19.3 us
    all_to_all x1, blocking collectives, body(): lax.all_to_all(packed.reshape(ep_count, capacity, sent_width), 'ep', spli...  12.8 us
    all_to_all x1, waiting for transfers between devices, body(): lax.all_to_all(expert_out.reshape(ep_count, capacity, own_width), 'ep', s...  6.86 us
    all_gather x1, blocking collectives, body(): expert_rows = lax.all_gather(expert_rows, 'tp', axis=1, tiled=True)  6.49 us
    psum x1, blocking collectives, body(): squares = lax.psum(jnp.sum(residual * residual, axis=-1), 'tp')  5.76 us
    dot_general x1, matrix products, body(): jnp.einsum('bkgl,bkdl->bkgd', past_prob.reshape(seq_count, kv_local, grou...  5.65 us
    all_to_all x1, starting transfers between devices, body(): lax.all_to_all(expert_out.reshape(ep_count, capacity, own_width), 'ep', s...  5.5 us
  transfers between devices with their start and end apart: 3, of which 3 were waited for; matrix products, arithmetic and copies ran while one was open for 1% of the time, Pallas kernels for 0%

commit v1 on v0

--- a/solution.py
+++ b/solution.py
@@ -88,7 +88,7 @@
         jnp.float32
     )
     residual = lax.dynamic_slice_in_dim(tokens_wide, column_start, own_width, 1) + attention
-    squares = lax.psum(jnp.sum(residual * residual, axis=-1), "tp")
+    squares = jnp.sum(lax.all_gather(jnp.sum(residual * residual, axis=-1), "tp"), axis=0)
     gain_part = lax.dynamic_slice_in_dim(post_gain, column_start, own_width, 0)
     expert_input = (residual * lax.rsqrt(squares / width + epsilon)[:, None] * gain_part).astype(
         jnp.bfloat16

time: 134 us -> 134 us (level)
    psum x1 -> x0, blocking collectives: 5.76 us -> none  [body(): squares = lax.psum(jnp.sum(residual * residual, axis=-1), 'tp')]
    unnamed x0 -> x1, blocking collectives: none -> 5.73 us
  transfers between devices with their start and end apart: 3 -> 3, of which waited for: 3 -> 3; matrix products, arithmetic and copies ran while one was open for 1% -> 2% of each run, Pallas kernels for 0% -> 0%
where the time goes in v1:
time: 134 us; the launch traced here: 133 us
  waiting for transfers between devices  46.1 us (34%)
  matrix products  27.8 us (21%)
  blocking collectives  25 us (19%)
  between operations  14.3 us (11%)
  other arithmetic  8.79 us (7%)
  local copies, waits for them, and re-layouts  5.73 us (4%)
  starting transfers between devices  5.55 us (4%)
    reduce_scatter x1, waiting for transfers between devices, body(): lax.psum_scatter(partial_value, 'tp', scatter_dimension=1, tiled=True)  19.9 us
    reduce_scatter x1, waiting for transfers between devices, body(): lax.psum_scatter(down_part, 'tp', scatter_dimension=1, tiled=True)  19.3 us
    all_to_all x1, blocking collectives, body(): lax.all_to_all(packed.reshape(ep_count, capacity, sent_width), 'ep', spli...  12.8 us
    all_to_all x1, waiting for transfers between devices, body(): lax.all_to_all(expert_out.reshape(ep_count, capacity, own_width), 'ep', s...  6.86 us
    all_gather x1, blocking collectives, body(): expert_rows = lax.all_gather(expert_rows, 'tp', axis=1, tiled=True)  6.49 us
    unnamed x1, blocking collectives  5.73 us
    dot_general x1, matrix products, body(): jnp.einsum('bkgl,bkdl->bkgd', past_prob.reshape(seq_count, kv_local, grou...  5.66 us
    all_to_all x1, starting transfers between devices, body(): lax.all_to_all(expert_out.reshape(ep_count, capacity, own_width), 'ep', s...  5.5 us
  transfers between devices with their start and end apart: 3, of which 3 were waited for; matrix products, arithmetic and copies ran while one was open for 2% of the time, Pallas kernels for 0%

profile of v1, /device:TPU:0, one launch (start us, length us, event | category | flops | bytes accessed | tf_op | source)
XLA Modules:
  0.0 133.3 jit_solution(3088765912253314386)
XLA Ops:
  6.5 0.0 copy-start
  6.5 0.0 reduce-scatter.3.cloned.1.call-start
  6.5 0.8 broadcast_add_fusion
  7.3 0.7 iota_compare_fusion.1
  8.1 1.0 multiply_reduce_fusion
  9.1 0.1 iota_compare_fusion
  9.2 1.5 %select_reduce_fusion = f32[32,8]{1,0:T(8,128)S(1)} fusion(f32[32,8,1024]{2,1,0:T(8,128)} %param.27, pred[32,1024]{1,0:T(8,128)(4,1)S(1)} %iota_compare_fusion), kind=kLoop, calls=%fused_computation.25 | loop fusion | flops 524032 | bytes 1082368 | tf_op jit(solution)/shard_map/reduce_sum | solution.py:59
  10.7 0.1 copy.36
  10.8 1.1 fusion.43
  11.9 0.1 copy.37
  12.0 2.2 %convolution_convert_fusion.2 = bf16[32,512]{1,0:T(8,128)(2,1)S(1)} fusion(bf16[2048,512]{1,0:T(8,128)(2,1)} %param.20, f32[2048]{0:T(1024)} %param.18, f32[32]{0:T(128)S(1)} %add_rsqrt_fusion.1, bf16[32,2048]{1,0:T(8,128)(2,1)} %param.17), kind=kOutput, calls=%fused_computation.16 | convolution fusion | flops 67387392 | bytes 2269312 | tf_op jit(solution)/shard_map/dot_general | solution.py:47
  14.2 0.1 reshape.173
  14.3 4.6 %convolution_multiply_fusion = f32[32,2,4,1024]{3,2,1,0:T(4,128)S(1)} fusion(bf16[32,2,4,64]{3,2,1,0:T(4,128)(2,1)S(1)} %reshape.173, bf16[32,2,64,1024]{3,2,1,0:T(8,128)(2,1)} %param.25), kind=kOutput, calls=%fused_computation.8 | convolution fusion | flops 33816576 | bytes 9469952 | tf_op jit(solution)/shard_map/bkgd,bkdl->bkgl/dot_general | solution.py:54
  18.9 0.0 copy-start.3
  18.9 1.4 %mul.121 = f32[32,8,1024]{2,1,0:T(8,128)} reshape(f32[32,2,4,1024]{3,2,1,0:T(4,128)S(1)} %convolution_multiply_fusion) | data formatting | bytes 2097152 | tf_op jit(solution)/shard_map/mul | solution.py:60
  20.3 1.9 %fusion.54 = (f32[32,8]{1,0:T(8,128)S(1)}, f32[32,8,1024]{2,1,0:T(8,128)S(1)}) fusion(f32[32,8,1024]{2,1,0:T(8,128)} %param.27, f32[32,8,1024]{2,1,0:T(8,128)} %mul.121, f32[32,8]{1,0:T(8,128)S(1)} %copy.37, pred[32,1024]{1,0:T(8,128)(4,1)S(1)} %iota_compare_fusion.1), kind=kLoop, calls=%fused_computation.81 | loop fusion | flops 1048320 | bytes 3180544 | tf_op jit(solution)/shard_map/reduce_max | solution.py:68
  22.2 0.1 copy.38
  22.2 1.3 convolution_convert_fusion.5
  23.5 0.1 reshape.192
  23.6 0.2 fusion.55
  23.8 0.1 copy.48
  23.9 0.1 copy.39
  24.0 0.3 fusion.18
  24.3 0.1 copy.40
  24.4 0.1 copy.41
  24.5 1.1 divide_convert_fusion
  25.6 1.2 reshape.175
  26.8 0.1 copy.44
  26.9 1.3 fusion.17
  28.2 0.1 reshape.182
  28.3 0.0 copy-start.5
  28.3 0.0 copy-start.6
  28.4 5.7 %fusion.15 = bf16[32,2,4,64]{3,2,1,0:T(4,128)(2,1)S(1)} fusion(bf16[32,2,4,1024]{3,2,1,0:T(4,128)(2,1)S(1)} %reshape.175, bf16[32,2,64,1024]{3,2,1,0:T(8,128)(2,1)} %param.26, f32[32,2,64]{2,1,0:T(2,128)S(1)} %reshape.182, f32[32,2,4]{2,1,0:T(2,128)S(1)} %copy.44), kind=kOutput, calls=%fused_computation.13 | convolution fusion | flops 33603584 | bytes 8963072 | tf_op jit(solution)/shard_map/bkgl,bkdl->bkgd/dot_general | solution.py:74
  34.0 0.1 reshape.176
  34.1 0.0 copy-done
  34.2 1.1 convolution_convert_fusion
  35.3 0.0 reduce-scatter.3.cloned.1.call-update
  35.3 0.0 reduce-scatter.5.cloned.1.call-start
  35.3 0.1 copy.45
  35.4 0.1 reshape.177
  35.5 0.1 fusion.31
  35.6 0.1 reduce_window_sum.11
  35.7 0.2 select_reduce_fusion.1
  35.9 0.6 dynamic-slice
  37.2 0.8 dynamic_slice.11
  38.0 19.9 %reduce-scatter.3.cloned.1.call-done = bf16[32,512]{1,0:T(8,128)(2,1)} async-done(((bf16[32,2048]{1,0:T(8,128)(2,1)}), bf16[32,512]{1,0:T(8,128)(2,1)}) %reduce-scatter.3.cloned.1.call-update) | async-done | bytes 32784 | tf_op jit(solution)/shard_map/reduce_scatter | solution.py:87
  57.9 0.9 multiply_reduce_fusion.1
  58.7 0.2 dynamic-update-slice
  59.0 5.7 %all-reduce = f32[128]{0:T(128)S(1)} all-reduce(f32[128]{0:T(128)S(1)} %dynamic-update-slice), channel_id=2, replica_groups=mesh['ep'=8,'tp'=4] {'tp'}, use_global_device_ids=true, to_apply=%add | all-reduce | flops 128 | bytes 1024
  64.7 0.1 reshape.183
  64.8 1.2 convolution_convert_fusion.1
  66.1 12.8 %all_to_all.10 = bf16[8,16,512]{2,1,0:T(8,128)(2,1)S(1)} all-to-all(bf16[8,16,512]{2,1,0:T(8,128)(2,1)S(1)} %bitcast.47), channel_id=1, replica_groups=mesh['ep'=8,'tp'=4] {'ep'}, dimensions={0} | all-to-all | bytes 262144 | tf_op jit(solution)/shard_map/all_to_all | solution.py:118
  78.9 6.5 %all_gather.11 = bf16[128,2048]{1,0:T(8,128)(2,1)S(1)} all-gather(bf16[128,512]{1,0:T(8,128)(2,1)S(1)} %bitcast.44), channel_id=1, replica_groups=mesh['ep'=8,'tp'=4] {'tp'}, dimensions={1}, use_global_device_ids=true | all-gather | bytes 655360 | tf_op jit(solution)/shard_map/all_gather | solution.py:126
  85.4 2.8 %fusion.4 = f32[128,896]{1,0:T(8,128)S(1)} fusion(bf16[128,2048]{1,0:T(8,128)(2,1)S(1)} %all_gather.11, bf16[1,2048,896]{2,1,0:T(8,128)(2,1)} %param.31), kind=kOutput, calls=%fused_computation.4 | convolution fusion | flops 469762048 | bytes 4653056 | tf_op jit(solution)/shard_map/dot_general | solution.py:127
  88.1 0.0 copy-start.4
  88.1 5.3 %fusion.6 = bf16[128,2048]{1,0:T(8,128)(2,1)} fusion(bf16[1,896,2048]{2,1,0:T(8,128)(2,1)} %param.33, bf16[128,2048]{1,0:T(8,128)(2,1)S(1)} %all_gather.11, bf16[1,2048,896]{2,1,0:T(8,128)(2,1)} %param.32, f32[128,896]{1,0:T(8,128)S(1)} %fusion.4), kind=kOutput, calls=%fused_computation.6 | convolution fusion | flops 940474368 | bytes 8847360 | tf_op jit(solution)/shard_map/dot_general | solution.py:130
  93.4 0.0 reduce-scatter.5.cloned.1.call-update
  93.5 19.3 %reduce-scatter.5.cloned.1.call-done = bf16[128,512]{1,0:T(8,128)(2,1)} async-done(((bf16[128,2048]{1,0:T(8,128)(2,1)}), bf16[128,512]{1,0:T(8,128)(2,1)}) %reduce-scatter.5.cloned.1.call-update) | async-done | bytes 131088 | tf_op jit(solution)/shard_map/reduce_scatter | solution.py:134
  112.8 5.5 %all-to-all-start.1 = ((bf16[8,16,512]{2,1,0:T(8,128)(2,1)}), bf16[8,16,512]{2,1,0:T(8,128)(2,1)S(1)}, u32[]{:S(2)}, u32[]{:S(2)}) async-start(bf16[8,16,512]{2,1,0:T(8,128)(2,1)} %bitcast.46), calls=%async_computation.3 | async-start | bytes 262144 | tf_op jit(solution)/shard_map/all_to_all | solution.py:138
  118.3 0.1 copy.46
  118.4 0.1 mul.132
  118.5 0.3 fusion.29
  118.7 6.9 %all-to-all-done.1 = bf16[8,16,512]{2,1,0:T(8,128)(2,1)S(1)} async-done(((bf16[8,16,512]{2,1,0:T(8,128)(2,1)}), bf16[8,16,512]{2,1,0:T(8,128)(2,1)S(1)}, u32[]{:S(2)}, u32[]{:S(2)}) %all-to-all-start.1) | async-done | bytes 131104 | tf_op jit(solution)/shard_map/all_to_all | solution.py:138
  125.6 0.8 fusion.16
  (21 shorter events, 0.2 us)
Async XLA Ops:
  6.5 27.6 %copy-start = (bf16[512,2048]{1,0:T(8,128)(2,1)S(1)}, bf16[512,2048]{1,0:T(8,128)(2,1)}, u32[]{:S(2)}) copy-start(bf16[512,2048]{1,0:T(8,128)(2,1)} %param.24) | copy-start | bytes 6291460
  6.5 51.3 %reduce-scatter.3.cloned.1.call-start = ((), (), s32[]{:S(2)}) async-start(), calls=%async_computation.4 | async-start | bytes 163840 | tf_op jit(solution)/shard_map/reduce_scatter | solution.py:87
  18.9 3.3 %copy-start.1 = (bf16[32,2048]{1,0:T(8,128)(2,1)S(1)}, bf16[32,2048]{1,0:T(8,128)(2,1)}, u32[]{:S(2)}) copy-start(bf16[32,2048]{1,0:T(8,128)(2,1)} %param.17) | copy-start | bytes 393220
  18.9 3.3 %copy-start.3 = (f32[2048]{0:T(1024)S(1)}, f32[2048]{0:T(1024)}, u32[]{:S(2)}) copy-start(f32[2048]{0:T(1024)} %param.18) | copy-start | bytes 24580
  28.3 7.0 %copy-start.5 = (s32[32,2]{0,1:T(2,128)S(1)}, s32[32,2]{0,1:T(2,128)}, u32[]{:S(2)}) copy-start(s32[32,2]{0,1:T(2,128)} %param.29) | copy-start | bytes 772
  28.3 7.6 %copy-start.6 = (u32[32]{0:T(128)S(1)}, u32[32]{0:T(128)}, u32[]{:S(2)}) copy-start(u32[32]{0:T(128)} %constant.69) | copy-start | bytes 388
  35.3 77.5 %reduce-scatter.5.cloned.1.call-start = ((), (), s32[]{:S(2)}) async-start(), calls=%async_computation.5 | async-start | bytes 655360 | tf_op jit(solution)/shard_map/reduce_scatter | solution.py:134
  88.1 5.3 %copy-start.4 = (f32[32,2]{0,1:T(2,128)S(1)}, f32[32,2]{0,1:T(2,128)}, u32[]{:S(2)}) copy-start(f32[32,2]{0,1:T(2,128)} %param.30) | copy-start | bytes 772
  88.1 37.5 %copy-start.2 = (bf16[32,512]{1,0:T(8,128)(2,1)S(1)}, bf16[32,512]{1,0:T(8,128)(2,1)}, u32[]{:S(2)}) copy-start(bf16[32,512]{1,0:T(8,128)(2,1)} %reduce-scatter.3.cloned.1.call-done) | copy-start | bytes 98308
  112.8 12.8 %all-to-all-start.1 = ((bf16[8,16,512]{2,1,0:T(8,128)(2,1)}), bf16[8,16,512]{2,1,0:T(8,128)(2,1)S(1)}, u32[]{:S(2)}, u32[]{:S(2)}) async-start(bf16[8,16,512]{2,1,0:T(8,128)(2,1)} %bitcast.46), calls=%async_computation.3 | async-start | bytes 262144 | tf_op jit(solution)/shard_map/all_to_all | solution.py:138
Sparse Core Ops, SparseCore 0:
  35.4 22.4 reduce-scatter.2
  93.6 19.1 reduce-scatter.4
